TPU v7x, 32 devices: a whole 2x2x4 slice. The times are simulated.
32 devices in a mesh: ep: 8 (over z, core), tp: 4 (over y, x).
Axes of the slice: x: 2, y: 2, z: 4, core: 2. Of those that a mesh axis runs over, the one named last changes fastest.
Arguments:
- resid: bfloat16 [32, 2048], P('ep', 'tp'), may hold values from -6 to 6
- cache_key: bfloat16 [32, 8, 224, 256], P(('ep', 'tp')), may hold values from -360 to 360
- cache_value: bfloat16 [32, 8, 224, 256], P(('ep', 'tp')), may hold values from -6 to 6
- lengths: int32 [32], P(('ep', 'tp')), may hold values from 28 to 224
- lambdas: float32 [8], replicated, may hold values from 0.3 to 0.8
- mix_gain: float32 [2048], replicated, may hold values from 0.1 to 1.9
- query_gain: float32 [128], replicated, may hold values from 0.1 to 1.9
- key_gain: float32 [128], replicated, may hold values from 0.1 to 1.9
- sub_gain: float32 [256], replicated, may hold values from 0.1 to 1.9
- ffn_gain: float32 [2048], replicated, may hold values from 0.1 to 1.9
- w_query: bfloat16 [2048, 2048], P(None, 'tp'), may hold values from -0.125 to 0.125
- w_key: bfloat16 [2048, 2048], P(None, 'tp'), may hold values from -0.125 to 0.125
- w_value: bfloat16 [2048, 2048], P(None, 'tp'), may hold values from -0.125 to 0.125
- w_out: bfloat16 [2048, 2048], P(None, 'tp'), may hold values from -0.125 to 0.125
- routes: int32 [32, 2], P('ep'), may hold values from 0 to 7, all different within a row; in each aligned block of 4 rows (0 to 3, 4 to 7, ...) at most 4 rows name the same one
- route_weights: float32 [32, 2], P('ep'), may hold values from 0.2 to 0.8
- w_gate: bfloat16 [8, 2048, 4096], P('ep', None, 'tp'), may hold values from -0.125 to 0.125
- w_up: bfloat16 [8, 2048, 4096], P('ep', None, 'tp'), may hold values from -0.125 to 0.125
- w_down: bfloat16 [8, 4096, 2048], P('ep', 'tp'), may hold values from -0.09375 to 0.09375
Outputs:
- result: bfloat16 [32, 2048], P('ep', 'tp')
- new_key: bfloat16 [32, 8, 256], P(('ep', 'tp'))
- new_value: bfloat16 [32, 8, 256], P(('ep', 'tp'))
Inputs may be any that keep to these rules, and one draw needn't show every extreme that they name: `routes`: within the 4 rows of one index of ep no expert is named more than 4 times, and in some of them one expert is named exactly 4 times; the two experts of a row differ. `lengths`: every sequence has at least two live positions.
All inputs are finite; a program needn't handle non-finite values.
Results may differ from a plain program's by a relative error of at most 0.0099.
Values may be sent and summed in bfloat16 or wider, within the bound.
A program may use at most 64 MiB of HBM per device.

v0:
```python
import math

import jax
import jax.numpy as jnp
from jax import lax
from jax.sharding import PartitionSpec as P

CAP = 4


epsilon = 1e-06
out_factor = 0.2 + 0.6 * math.exp(-0.3)
masked_score = -1e30


def scaled_rows(values, gain):
    wide = values.astype(jnp.float32)
    return wide * lax.rsqrt(jnp.mean(wide * wide, axis=-1, keepdims=True) + epsilon) * gain


def route_tables(routes, route_weights, experts, capacity):
    flat_routes = routes.reshape(-1)
    expert_hit = (flat_routes[:, None] == jnp.arange(experts, dtype=jnp.int32)[None, :]).astype(
        jnp.int32
    )
    before = jnp.cumsum(expert_hit, axis=0) - expert_hit
    slot_index = jnp.sum(before * expert_hit, axis=1)
    slot_hit = (slot_index[:, None] == jnp.arange(capacity, dtype=jnp.int32)[None, :]).astype(
        jnp.float32
    )
    pair_table = expert_hit.astype(jnp.float32)[:, :, None] * slot_hit[:, None, :]
    pair_table = pair_table.reshape(routes.shape[0], 2, experts, capacity)
    dispatch = jnp.sum(pair_table, axis=1)
    combine = jnp.sum(pair_table * route_weights[:, :, None, None], axis=1)
    return (dispatch, combine)


def attend(
    queries,
    key_rows,
    value_rows,
    past_keys,
    past_values,
    live_len,
    lambdas,
    query_gain,
    key_gain,
    sub_gain,
):
    seq_count, kv_heads, cache_len, key_width = past_keys.shape
    head_dim = key_width // 2
    head_count = lambdas.shape[0]
    group_size = head_count // kv_heads
    value_dim = past_values.shape[-1]
    score_scale = head_dim ** (-0.5)
    q_unit = scaled_rows(
        queries.reshape(seq_count, kv_heads, group_size, 2, head_dim), query_gain
    ).astype(jnp.bfloat16)
    new_key = scaled_rows(key_rows.reshape(seq_count, kv_heads, 2, head_dim), key_gain).astype(
        jnp.bfloat16
    )
    new_value = value_rows.reshape(seq_count, kv_heads, value_dim)
    past_split = past_keys.reshape(seq_count, kv_heads, cache_len, 2, head_dim)
    scores = (
        jnp.einsum("sjgmd,sjlmd->sjgml", q_unit, past_split, preferred_element_type=jnp.float32)
        * score_scale
    )
    own_score = (
        jnp.einsum("sjgmd,sjmd->sjgm", q_unit, new_key, preferred_element_type=jnp.float32)
        * score_scale
    )
    live_mask = jnp.arange(cache_len, dtype=jnp.int32)[None, :] < live_len[:, None]
    scores = jnp.where(live_mask[:, None, None, None, :], scores, masked_score)
    peak = jnp.maximum(jnp.max(scores, axis=-1), own_score)
    past_weight = jnp.exp(scores - peak[..., None])
    own_weight = jnp.exp(own_score - peak)
    totals = jnp.sum(past_weight, axis=-1) + own_weight
    past_prob = past_weight / totals[..., None]
    own_prob = own_weight / totals
    mix_lambda = lambdas.reshape(1, kv_heads, group_size, 1)
    past_mix = (past_prob[..., 0, :] - mix_lambda * past_prob[..., 1, :]).astype(jnp.bfloat16)
    own_mix = (own_prob[..., 0] - mix_lambda[..., 0] * own_prob[..., 1]).astype(jnp.bfloat16)
    head_out = jnp.einsum(
        "sjgl,sjlv->sjgv", past_mix, past_values, preferred_element_type=jnp.float32
    )
    head_out = (
        head_out
        + own_mix.astype(jnp.float32)[..., None] * new_value.astype(jnp.float32)[:, :, None, :]
    )
    mixed = (
        (scaled_rows(head_out, sub_gain) * out_factor)
        .astype(jnp.bfloat16)
        .reshape(seq_count, head_count * value_dim)
    )
    return (mixed, new_key.reshape(seq_count, kv_heads, key_width), new_value)


def local(
    resid,
    cache_key,
    cache_value,
    lengths,
    lambdas,
    mix_gain,
    query_gain,
    key_gain,
    sub_gain,
    ffn_gain,
    w_query,
    w_key,
    w_value,
    w_out,
    routes,
    route_weights,
    w_gate,
    w_up,
    w_down,
):
    gathered = lax.all_gather(resid, "tp", axis=1, tiled=True)
    normed = scaled_rows(gathered, mix_gain).astype(jnp.bfloat16)
    query_part = jnp.dot(normed, w_query, preferred_element_type=jnp.float32).astype(jnp.bfloat16)
    key_part = jnp.dot(normed, w_key, preferred_element_type=jnp.float32).astype(jnp.bfloat16)
    value_part = jnp.dot(normed, w_value, preferred_element_type=jnp.float32).astype(jnp.bfloat16)
    queries, key_rows, value_rows = (
        lax.all_to_all(query_part, "tp", split_axis=0, concat_axis=1, tiled=True),
        lax.all_to_all(key_part, "tp", split_axis=0, concat_axis=1, tiled=True),
        lax.all_to_all(value_part, "tp", split_axis=0, concat_axis=1, tiled=True),
    )
    mixed, new_key, new_value = attend(
        queries,
        key_rows,
        value_rows,
        cache_key,
        cache_value,
        lengths,
        lambdas,
        query_gain,
        key_gain,
        sub_gain,
    )
    attn_proj = jnp.dot(
        lax.all_gather(mixed, "tp", axis=0, tiled=True), w_out, preferred_element_type=jnp.float32
    )
    updated = (resid.astype(jnp.float32) + attn_proj).astype(jnp.bfloat16)
    updated_rows = lax.all_gather(updated, "tp", axis=1, tiled=True)
    hidden = scaled_rows(updated_rows, ffn_gain).astype(jnp.bfloat16)
    experts = w_gate.shape[0] * lax.axis_size("ep")
    dispatch, combine = route_tables(routes, route_weights, experts, CAP)
    send = jnp.einsum(
        "gec,gd->ecd", dispatch.astype(jnp.bfloat16), hidden, preferred_element_type=jnp.float32
    ).astype(jnp.bfloat16)
    slots = lax.all_to_all(send, "ep", split_axis=0, concat_axis=0, tiled=True)
    flat_rows = slots.reshape(-1, slots.shape[-1])
    gate_out = jnp.dot(flat_rows, w_gate[0], preferred_element_type=jnp.float32)
    up_out = jnp.dot(flat_rows, w_up[0], preferred_element_type=jnp.float32)
    act = (jax.nn.silu(gate_out) * up_out).astype(jnp.bfloat16)
    down_out = jnp.dot(act, w_down[0], preferred_element_type=jnp.float32)
    partial_value = down_out.reshape(slots.shape[0], slots.shape[1], down_out.shape[-1])
    flat_combine = combine.reshape(combine.shape[0], -1)
    summed = lax.psum_scatter(
        partial_value.astype(jnp.bfloat16), "tp", scatter_dimension=2, tiled=True
    ).astype(jnp.float32)
    returned = lax.all_to_all(
        summed.astype(jnp.bfloat16), "ep", split_axis=0, concat_axis=0, tiled=True
    ).astype(summed.dtype)
    expert_mix = jnp.dot(
        flat_combine,
        returned.reshape(-1, returned.shape[-1]),
        precision=lax.Precision.HIGHEST,
        preferred_element_type=jnp.float32,
    )
    result = (updated.astype(jnp.float32) + expert_mix).astype(jnp.bfloat16)
    return (result, new_key, new_value)


def solution(mesh):
    in_specs = (
        P("ep", "tp"),
        P(("ep", "tp"), None, None, None),
        P(("ep", "tp"), None, None, None),
        P(("ep", "tp")),
        P(),
        P(),
        P(),
        P(),
        P(),
        P(),
        P(None, "tp"),
        P(None, "tp"),
        P(None, "tp"),
        P(None, "tp"),
        P("ep", None),
        P("ep", None),
        P("ep", None, "tp"),
        P("ep", None, "tp"),
        P("ep", "tp", None),
    )
    out_specs = (P("ep", "tp"), P(("ep", "tp"), None, None), P(("ep", "tp"), None, None))
    return jax.shard_map(local, mesh=mesh, in_specs=in_specs, out_specs=out_specs, check_vma=False)
```

profile of v0, /device:TPU:0, one launch (start us, length us, event | category | flops | bytes accessed | tf_op | source)
XLA Modules:
  0.0 129.9 jit_solution(2296652605895860037)
XLA Ops:
  7.2 0.0 copy-start
  7.2 9.9 %all_gather.9 = bf16[4,2048]{1,0:T(4,128)(2,1)S(1)} all-gather(bf16[4,512]{1,0:T(4,128)(2,1)} %param.19), channel_id=1, replica_groups=mesh['ep'=8,'tp'=4] {'tp'}, dimensions={1}, use_global_device_ids=true | all-gather | bytes 20480 | tf_op jit(solution)/shard_map/all_gather | solution.py:119
  17.1 0.1 fusion.26
  17.3 1.1 fusion.18
  18.4 0.5 broadcast.214
  18.9 0.7 reduce.19
  19.6 0.6 reshape.382
  20.2 3.2 %all-to-all-start = ((bf16[4,2,256]{2,1,0:T(2,128)(2,1)}), bf16[4,2,256]{2,1,0:T(2,128)(2,1)S(1)}, u32[]{:S(2)}, u32[]{:S(2)}) async-start(bf16[4,2,256]{2,1,0:T(2,128)(2,1)} %reshape.382), calls=%async_computation | async-start | bytes 8192 | tf_op jit(solution)/shard_map/all_to_all | solution.py:125
  23.4 0.1 copy.64
  23.5 0.1 eq.47
  23.6 0.1 fusion.48
  23.7 2.1 %fusion.19 = bf16[4,1,512]{2,0,1:T(4,128)(2,1)S(1)} fusion(bf16[2048,512]{1,0:T(8,128)(2,1)} %param.30, bf16[4,2048]{1,0:T(4,128)(2,1)S(1)} %all_gather.9, f32[2048]{0:T(1024)S(1)} %copy-done.3, f32[4]{0:T(128)S(1)} %add_rsqrt_fusion.4), kind=kOutput, calls=%fused_computation.19 | convolution fusion | flops 8423424 | bytes 2125840 | tf_op jit(solution)/shard_map/dot_general | solution.py:122
  26.5 0.0 copy-start.10
  26.5 0.0 copy-start.11
  26.5 0.4 fusion.20
  27.0 0.1 fusion.51
  27.1 0.2 select_reduce_fusion
  27.2 0.1 eq.51
  27.3 0.1 compare_convert_fusion
  27.4 0.1 copy.66
  27.5 0.1 multiply_reduce_fusion
  27.6 0.7 reduce.18
  28.3 0.6 reshape.384
  28.9 2.2 %reshape.356 = bf16[8,224,2,128]{3,2,1,0:T(2,128)(2,1)S(1)} reshape(bf16[1,8,224,256]{3,2,1,0:T(8,128)(2,1)} %param.20) | data formatting | bytes 1835008 | tf_op jit(solution)/shard_map/reshape.7
  31.1 0.7 reduce.17
  31.7 0.6 reshape.380
  32.3 4.2 %all-to-all-start.1 = ((bf16[4,2,256]{2,1,0:T(2,128)(2,1)}), bf16[4,2,256]{2,1,0:T(2,128)(2,1)S(1)}, u32[]{:S(2)}, u32[]{:S(2)}) async-start(bf16[4,2,256]{2,1,0:T(2,128)(2,1)} %reshape.384), calls=%async_computation.1 | async-start | bytes 8192 | tf_op jit(solution)/shard_map/all_to_all | solution.py:126
  36.5 4.6 %all-to-all-done.1 = bf16[4,2,256]{2,1,0:T(2,128)(2,1)S(1)} async-done(((bf16[4,2,256]{2,1,0:T(2,128)(2,1)}), bf16[4,2,256]{2,1,0:T(2,128)(2,1)S(1)}, u32[]{:S(2)}, u32[]{:S(2)}) %all-to-all-start.1) | async-done | bytes 4128 | tf_op jit(solution)/shard_map/all_to_all | solution.py:126
  41.2 3.2 %all-to-all-start.2 = ((bf16[4,2,256]{2,1,0:T(2,128)(2,1)}), bf16[4,2,256]{2,1,0:T(2,128)(2,1)S(1)}, u32[]{:S(2)}, u32[]{:S(2)}) async-start(bf16[4,2,256]{2,1,0:T(2,128)(2,1)} %reshape.380), calls=%async_computation.2 | async-start | bytes 8192 | tf_op jit(solution)/shard_map/all_to_all | solution.py:127
  44.4 0.0 reduce-scatter.2.cloned.1.call-start
  44.6 0.1 reduce_sum.83
  44.6 0.1 reduce_sum.82
  44.8 0.2 fusion.45
  44.9 0.1 copy.79
  45.0 0.6 fusion.23
  45.6 0.1 fusion.41
  45.7 0.2 fusion.40
  45.9 0.1 divide_bitcast_fusion
  46.0 0.1 fusion.49
  46.1 3.0 %all-to-all-done.2 = bf16[4,2,256]{2,1,0:T(2,128)(2,1)S(1)} async-done(((bf16[4,2,256]{2,1,0:T(2,128)(2,1)}), bf16[4,2,256]{2,1,0:T(2,128)(2,1)S(1)}, u32[]{:S(2)}, u32[]{:S(2)}) %all-to-all-start.2) | async-done | bytes 4128 | tf_op jit(solution)/shard_map/all_to_all | solution.py:127
  49.1 1.4 %fusion.21 = f32[8,1,256]{2,1,0:T(1,128)S(1)} fusion(bf16[1,8,224,256]{3,2,1,0:T(8,128)(2,1)} %param.21, bf16[8,224,1]{1,0,2:T(8,128)(2,1)S(1)} %fusion.49), kind=kOutput, calls=%fused_computation.21 | convolution fusion | flops 917504 | bytes 929280 | tf_op jit(solution)/shard_map/sjgl,sjlv->sjgv/dot_general | solution.py:83
  50.5 0.2 multiply_reduce_fusion.1
  50.8 0.1 multiply_convert_fusion.1
  50.8 7.2 %all-gather = bf16[4,1,2048]{2,1,0:T(2,128)(2,1)S(1)} all-gather(bf16[1,1,2048]{2,1,0:T(2,128)(2,1)S(1)} %reshape.365), channel_id=1, replica_groups=mesh['ep'=8,'tp'=4] {'tp'}, dimensions={0}, use_global_device_ids=true | all-gather | bytes 20480 | tf_op jit(solution)/shard_map/all_gather | solution.py:142
  58.1 2.0 %fusion.15 = bf16[4,512]{1,0:T(4,128)(2,1)S(1)} fusion(bf16[2048,512]{1,0:T(8,128)(2,1)} %param.32, bf16[4,1,2048]{2,1,0:T(2,128)(2,1)S(1)} %all-gather, bf16[4,512]{1,0:T(4,128)(2,1)S(1)} %copy-done.4), kind=kOutput, calls=%fused_computation.12 | convolution fusion | flops 8394752 | bytes 2121728 | tf_op jit(solution)/shard_map/dot_general | solution.py:141
  60.1 8.1 %all_gather.11 = bf16[4,2048]{1,0:T(4,128)(2,1)S(1)} all-gather(bf16[4,512]{1,0:T(4,128)(2,1)S(1)} %fusion.15), channel_id=1, replica_groups=mesh['ep'=8,'tp'=4] {'tp'}, dimensions={1}, use_global_device_ids=true | all-gather | bytes 20480 | tf_op jit(solution)/shard_map/all_gather | solution.py:145
  68.2 0.1 fusion.29
  68.3 0.2 convolution_convert_fusion
  68.6 0.1 copy.68
  68.7 11.4 %all_to_all.49 = bf16[8,4,2048]{2,1,0:T(4,128)(2,1)S(1)} all-to-all(bf16[8,4,2048]{2,1,0:T(4,128)(2,1)S(1)} %copy.68), channel_id=1, replica_groups=mesh['ep'=8,'tp'=4] {'ep'}, dimensions={0} | all-to-all | bytes 262144 | tf_op jit(solution)/shard_map/all_to_all | solution.py:152
  80.2 3.2 %fusion.4 = f32[32,1024]{1,0:T(8,128)S(1)} fusion(bf16[32,2048]{1,0:T(8,128)(2,1)S(1)} %reshape.359, bf16[1,2048,1024]{2,1,0:T(8,128)(2,1)} %param.35), kind=kOutput, calls=%fused_computation.4 | convolution fusion | flops 134217728 | bytes 4456448 | tf_op jit(solution)/shard_map/dot_general | solution.py:154
  83.3 0.3 copy-done.1
  83.6 0.8 fusion.12
  84.5 3.6 %fusion.6 = bf16[8,4,2048]{2,0,1:T(8,128)(2,1)} fusion(bf16[1,1024,2048]{2,1,0:T(8,128)(2,1)} %param.37, bf16[8,4,1024]{2,1,0:T(4,128)(2,1)S(1)} %dot_general.48), kind=kOutput, calls=%fused_computation.6 | convolution fusion | flops 134283264 | bytes 4390912 | tf_op jit(solution)/shard_map/dot_general | solution.py:157
  88.1 0.0 reduce-scatter.2.cloned.1.call-update
  88.1 0.1 copy.82
  88.2 0.1 mul.249
  88.3 22.2 %reduce-scatter.2.cloned.1.call-done = bf16[8,4,512]{2,0,1:T(8,128)(2,1)} async-done(((bf16[8,4,2048]{2,0,1:T(8,128)(2,1)}), bf16[8,4,512]{2,0,1:T(8,128)(2,1)}) %reduce-scatter.2.cloned.1.call-update) | async-done | bytes 32784 | tf_op jit(solution)/shard_map/reduce_scatter | solution.py:160
  110.5 1.4 %copy.70 = bf16[8,4,512]{2,1,0:T(4,128)(2,1)} copy(bf16[8,4,512]{2,0,1:T(8,128)(2,1)} %reduce-scatter.2.cloned.1.call-done) | data formatting | bytes 65536 | tf_op jit(solution)/shard_map/reduce_scatter | solution.py:160
  111.9 4.6 %all-to-all-start.4 = ((bf16[8,4,512]{2,1,0:T(4,128)(2,1)}), bf16[8,4,512]{2,1,0:T(4,128)(2,1)S(1)}, u32[]{:S(2)}, u32[]{:S(2)}) async-start(bf16[8,4,512]{2,1,0:T(4,128)(2,1)} %copy.70), calls=%async_computation.5 | async-start | bytes 65536 | tf_op jit(solution)/shard_map/all_to_all | solution.py:163
  116.5 0.6 multiply_convert_fusion
  117.1 0.6 reshape.360
  117.7 4.5 %all-to-all-done.4 = bf16[8,4,512]{2,1,0:T(4,128)(2,1)S(1)} async-done(((bf16[8,4,512]{2,1,0:T(4,128)(2,1)}), bf16[8,4,512]{2,1,0:T(4,128)(2,1)S(1)}, u32[]{:S(2)}, u32[]{:S(2)}) %all-to-all-start.4) | async-done | bytes 32800 | tf_op jit(solution)/shard_map/all_to_all | solution.py:163
  122.2 0.8 fusion.17
  (46 shorter events, 0.4 us)
Async XLA Ops:
  7.2 10.1 %copy-start = (bf16[2048,512]{1,0:T(8,128)(2,1)S(1)}, bf16[2048,512]{1,0:T(8,128)(2,1)}, u32[]{:S(2)}) copy-start(bf16[2048,512]{1,0:T(8,128)(2,1)} %param.29) | copy-start | bytes 6291460
  7.2 16.5 %copy-start.3 = (f32[2048]{0:T(1024)S(1)}, f32[2048]{0:T(1024)}, u32[]{:S(2)}) copy-start(f32[2048]{0:T(1024)} %param.24) | copy-start | bytes 24580
  7.2 16.2 %copy-start.7 = (s32[4,2]{0,1:T(2,128)S(1)}, s32[4,2]{0,1:T(2,128)}, u32[]{:S(2)}) copy-start(s32[4,2]{0,1:T(2,128)} %param.33) | copy-start | bytes 100
  20.2 12.2 %all-to-all-start = ((bf16[4,2,256]{2,1,0:T(2,128)(2,1)}), bf16[4,2,256]{2,1,0:T(2,128)(2,1)S(1)}, u32[]{:S(2)}, u32[]{:S(2)}) async-start(bf16[4,2,256]{2,1,0:T(2,128)(2,1)} %reshape.382), calls=%async_computation | async-start | bytes 8192 | tf_op jit(solution)/shard_map/all_to_all | solution.py:125
  23.6 2.9 %copy-start.2 = (bf16[2048,512]{1,0:T(8,128)(2,1)S(1)}, bf16[2048,512]{1,0:T(8,128)(2,1)}, u32[]{:S(2)}) copy-start(bf16[2048,512]{1,0:T(8,128)(2,1)} %param.31) | copy-start | bytes 6291460
  23.7 3.7 %copy-start.8 = (f32[4,2]{0,1:T(2,128)S(1)}, f32[4,2]{0,1:T(2,128)}, u32[]{:S(2)}) copy-start(f32[4,2]{0,1:T(2,128)} %param.34) | copy-start | bytes 100
  26.5 18.2 %copy-start.10 = (f32[128]{0:T(128)S(1)}, f32[128]{0:T(128)}, u32[]{:S(2)}) copy-start(f32[128]{0:T(128)} %param.25) | copy-start | bytes 1540
  26.5 18.2 %copy-start.11 = (f32[128]{0:T(128)S(1)}, f32[128]{0:T(128)}, u32[]{:S(2)}) copy-start(f32[128]{0:T(128)} %param.26) | copy-start | bytes 1540
  27.0 19.0 %copy-start.6 = (f32[8]{0:T(128)S(1)}, f32[8]{0:T(128)}, u32[]{:S(2)}) copy-start(f32[8]{0:T(128)} %param.23) | copy-start | bytes 100
  27.0 23.8 %copy-start.9 = (f32[256]{0:T(256)S(1)}, f32[256]{0:T(256)}, u32[]{:S(2)}) copy-start(f32[256]{0:T(256)} %param.27) | copy-start | bytes 3076
  28.9 29.2 %copy-start.4 = (bf16[4,512]{1,0:T(4,128)(2,1)S(1)}, bf16[4,512]{1,0:T(4,128)(2,1)}, u32[]{:S(2)}) copy-start(bf16[4,512]{1,0:T(4,128)(2,1)} %param.19) | copy-start | bytes 12292
  32.3 8.8 %all-to-all-start.1 = ((bf16[4,2,256]{2,1,0:T(2,128)(2,1)}), bf16[4,2,256]{2,1,0:T(2,128)(2,1)S(1)}, u32[]{:S(2)}, u32[]{:S(2)}) async-start(bf16[4,2,256]{2,1,0:T(2,128)(2,1)} %reshape.384), calls=%async_computation.1 | async-start | bytes 8192 | tf_op jit(solution)/shard_map/all_to_all | solution.py:126
  41.2 7.9 %all-to-all-start.2 = ((bf16[4,2,256]{2,1,0:T(2,128)(2,1)}), bf16[4,2,256]{2,1,0:T(2,128)(2,1)S(1)}, u32[]{:S(2)}, u32[]{:S(2)}) async-start(bf16[4,2,256]{2,1,0:T(2,128)(2,1)} %reshape.380), calls=%async_computation.2 | async-start | bytes 8192 | tf_op jit(solution)/shard_map/all_to_all | solution.py:127
  44.4 66.1 %reduce-scatter.2.cloned.1.call-start = ((), (), s32[]{:S(2)}) async-start(), calls=%async_computation.6 | async-start | bytes 163840 | tf_op jit(solution)/shard_map/reduce_scatter | solution.py:160
  45.0 23.3 %copy-start.5 = (f32[2048]{0:T(1024)S(1)}, f32[2048]{0:T(1024)}, u32[]{:S(2)}) copy-start(f32[2048]{0:T(1024)} %param.28) | copy-start | bytes 24580
  80.2 3.5 %copy-start.1 = (bf16[1,2048,1024]{2,1,0:T(8,128)(2,1)S(1)}, bf16[1,2048,1024]{2,1,0:T(8,128)(2,1)}, u32[]{:S(2)}) copy-start(bf16[1,2048,1024]{2,1,0:T(8,128)(2,1)} %param.36) | copy-start | bytes 12582916
  111.9 10.3 %all-to-all-start.4 = ((bf16[8,4,512]{2,1,0:T(4,128)(2,1)}), bf16[8,4,512]{2,1,0:T(4,128)(2,1)S(1)}, u32[]{:S(2)}, u32[]{:S(2)}) async-start(bf16[8,4,512]{2,1,0:T(4,128)(2,1)} %copy.70), calls=%async_computation.5 | async-start | bytes 65536 | tf_op jit(solution)/shard_map/all_to_all | solution.py:163
Sparse Core Ops, SparseCore 0:
  88.2 22.2 reduce-scatter.1
where the time goes:
time: 131 us; the launch traced here: 130 us
  blocking collectives  36.7 us (28%)
  waiting for transfers between devices  34.4 us (26%)
  matrix products  16.3 us (12%)
  starting transfers between devices  15.3 us (12%)
  between operations  15 us (11%)
  local copies, waits for them, and re-layouts  7.69 us (6%)
  other arithmetic  4.59 us (4%)
    reduce_scatter x1, waiting for transfers between devices, local(): lax.psum_scatter(partial_value.astype(jnp.bfloat16), 'tp', scatter_dimens...  22.2 us
    all_to_all x1, blocking collectives, local(): slots = lax.all_to_all(send, 'ep', split_axis=0, concat_axis=0, tiled=True)  11.4 us
    all_gather x1, blocking collectives, local(): gathered = lax.all_gather(resid, 'tp', axis=1, tiled=True)  9.93 us
    all_gather x1, blocking collectives, local(): updated_rows = lax.all_gather(updated, 'tp', axis=1, tiled=True)  8.12 us
    all_gather x1, blocking collectives, local(): lax.all_gather(mixed, 'tp', axis=0, tiled=True)  7.25 us
    all_to_all x1, waiting for transfers between devices, local(): lax.all_to_all(key_part, 'tp', split_axis=0, concat_axis=1, tiled=True)  4.63 us
    all_to_all x1, starting transfers between devices, local(): lax.all_to_all(summed.astype(jnp.bfloat16), 'ep', split_axis=0, concat_ax...  4.6 us
    all_to_all x1, waiting for transfers between devices, local(): lax.all_to_all(summed.astype(jnp.bfloat16), 'ep', split_axis=0, concat_ax...  4.51 us
  transfers between devices with their start and end apart: 5, of which 4 were waited for; matrix products, arithmetic and copies ran while one was open for 9% of the time, Pallas kernels for 0%

commit v1 on v0

--- a/solution.py
+++ b/solution.py
@@ -1,8 +1,11 @@
+import functools
 import math
 
 import jax
 import jax.numpy as jnp
 from jax import lax
+from jax.experimental import pallas as pl
+from jax.experimental.pallas import tpu as pltpu
 from jax.sharding import PartitionSpec as P
 
 CAP = 4
@@ -173,6 +176,482 @@
     return (result, new_key, new_value)
 
 
+MESH = pl.DeviceIdType.MESH
+
+
+def rms_scale(wide):
+    return lax.rsqrt(jnp.mean(wide * wide, axis=-1, keepdims=True) + epsilon)
+
+
+def fused(
+    n_ep,
+    n_tp,
+    lengths,
+    lambdas,
+    resid,
+    mix_gain,
+    query_gain,
+    key_gain,
+    sub_gain,
+    ffn_gain,
+    routes,
+    route_weights,
+    w_query,
+    w_key,
+    w_value,
+    cache_key,
+    cache_value,
+    w_out,
+    w_gate,
+    w_up,
+    w_down,
+    result,
+    new_key,
+    new_value,
+    mix_gain_v,
+    query_gain_v,
+    key_gain_v,
+    sub_gain_v,
+    ffn_gain_v,
+    routes_v,
+    weights_v,
+    wq_v,
+    wk_v,
+    wv_v,
+    ck_v,
+    cv_v,
+    wo_v,
+    wg_v,
+    wu_v,
+    wd_v,
+    res_all,
+    proj_send,
+    proj_all,
+    heads_v,
+    mix_all,
+    upd_all,
+    rows_v,
+    part_send,
+    part_all,
+    result_v,
+    new_key_v,
+    new_value_v,
+    load_sem,
+    out_sem,
+    res_s,
+    res_r,
+    proj_s,
+    proj_r,
+    mix_s,
+    mix_r,
+    upd_s,
+    upd_r,
+    part_s,
+    part_r,
+):
+    f32, bf16 = jnp.float32, jnp.bfloat16
+    ep, tp = lax.axis_index("ep"), lax.axis_index("tp")
+    count = n_ep * n_tp
+    me = ep * n_tp + tp
+    group, width = resid.shape
+    kv_heads, cache_len, key_width = ck_v.shape
+    head_dim = key_width // 2
+    heads_here = width // key_width
+
+    loads = [
+        (resid, res_all.at[tp]),
+        (mix_gain, mix_gain_v),
+        (w_query, wq_v),
+        (w_key, wk_v),
+        (w_value, wv_v),
+        (query_gain, query_gain_v),
+        (key_gain, key_gain_v),
+        (sub_gain, sub_gain_v),
+        (ffn_gain, ffn_gain_v),
+        (routes, routes_v),
+        (route_weights, weights_v),
+        (cache_key.at[0], ck_v),
+        (cache_value.at[0], cv_v),
+        (w_out, wo_v),
+        (w_gate.at[0], wg_v),
+        (w_up.at[0], wu_v),
+        (w_down.at[0], wd_v),
+    ]
+    copies = [
+        pltpu.make_async_copy(source, target, load_sem.at[at])
+        for at, (source, target) in enumerate(loads)
+    ]
+    for copy in copies:
+        copy.start()
+    (
+        resid_c,
+        mix_gain_c,
+        wq_c,
+        wk_c,
+        wv_c,
+        query_gain_c,
+        key_gain_c,
+        sub_gain_c,
+        ffn_gain_c,
+        routes_c,
+        weights_c,
+        ck_c,
+        cv_c,
+        wo_c,
+        wg_c,
+        wu_c,
+        wd_c,
+    ) = copies
+
+    barrier = pltpu.get_barrier_semaphore()
+
+    def greet(step, carry):
+        other = lax.rem(me + step, count)
+        pl.semaphore_signal(
+            barrier,
+            inc=1,
+            device_id=(other // n_tp, lax.rem(other, n_tp)),
+            device_id_type=MESH,
+        )
+        return carry
+
+    lax.fori_loop(1, count, greet, 0)
+    pl.semaphore_wait(barrier, count - 1)
+
+    def tp_copy(step, source, target, send, recv):
+        peer = lax.rem(tp + step, n_tp)
+        return pltpu.make_async_remote_copy(
+            src_ref=source(peer),
+            dst_ref=target.at[tp],
+            send_sem=send.at[step],
+            recv_sem=recv.at[tp],
+            device_id=(ep, peer),
+            device_id_type=MESH,
+        )
+
+    def tp_wait(step, target, send, recv):
+        peer = lax.rem(tp + step, n_tp)
+        return pltpu.make_async_remote_copy(
+            src_ref=target.at[peer],
+            dst_ref=target.at[peer],
+            send_sem=send.at[step],
+            recv_sem=recv.at[peer],
+            device_id=(ep, peer),
+            device_id_type=MESH,
+        )
+
+    resid_c.wait()
+    for step in range(1, n_tp):
+        tp_copy(step, lambda peer: res_all.at[tp], res_all, res_s, res_r).start()
+    mix_gain_c.wait()
+    for step in range(1, n_tp):
+        tp_wait(step, res_all, res_s, res_r).wait_recv()
+    wide = jnp.concatenate([res_all[t].astype(f32) for t in range(n_tp)], axis=1)
+    normed = (wide * rms_scale(wide) * mix_gain_v[...]).astype(bf16)
+
+    blocks = 2 * heads_here
+    for section, (copy, weight) in enumerate(((wq_c, wq_v), (wk_c, wk_v), (wv_c, wv_v))):
+        copy.wait()
+        out = jnp.dot(normed, weight[...], preferred_element_type=f32).astype(bf16).astype(f32)
+        for head in range(heads_here):
+            for half in range(2):
+                at = (head * 2 + half) * head_dim
+                proj_send[:, section * blocks + half * heads_here + head, :] = out[
+                    :, at : at + head_dim
+                ]
+    for step in range(1, n_tp):
+        tp_copy(step, lambda peer: proj_send.at[peer], proj_all, proj_s, proj_r).start()
+    proj_all[tp] = proj_send[tp]
+    for copy in (query_gain_c, key_gain_c, sub_gain_c, ffn_gain_c, routes_c, weights_c):
+        copy.wait()
+    for step in range(1, n_tp):
+        tp_wait(step, proj_all, proj_s, proj_r).wait_recv()
+    for t in range(n_tp):
+        for section in range(3):
+            for half in range(2):
+                at = section * blocks + half * heads_here
+                heads_v[section, half, t * heads_here : (t + 1) * heads_here, :] = proj_all[
+                    t, at : at + heads_here, :
+                ]
+    maps = 2 * kv_heads
+    q_raw = heads_v[0].reshape(maps, head_dim)
+    k_raw = heads_v[1].reshape(maps, head_dim)
+    q_unit = (q_raw * rms_scale(q_raw) * query_gain_v[...]).astype(bf16).astype(f32)
+    k_unit = (k_raw * rms_scale(k_raw) * key_gain_v[...]).astype(bf16).astype(f32)
+    value_own = jnp.concatenate([heads_v[2, 0], heads_v[2, 1]], axis=1)
+    new_key_v[...] = jnp.concatenate([k_unit[:kv_heads], k_unit[kv_heads:]], axis=1).astype(bf16)
+    new_value_v[...] = value_own.astype(bf16)
+    out_copies = [
+        pltpu.make_async_copy(new_key_v, new_key.at[0], out_sem.at[0]),
+        pltpu.make_async_copy(new_value_v, new_value.at[0], out_sem.at[1]),
+    ]
+    for copy in out_copies:
+        copy.start()
+
+    row = lax.broadcasted_iota(jnp.int32, (maps, 1), 0)
+    head_row = lax.rem(row, kv_heads)
+    first = row < kv_heads
+    q_wide = jnp.concatenate(
+        [jnp.where(first, q_unit, 0.0), jnp.where(first, 0.0, q_unit)], axis=1
+    ).astype(bf16)
+    ck_c.wait()
+    scores = jnp.zeros((maps, cache_len), f32)
+    for head in range(kv_heads):
+        part = lax.dot_general(
+            q_wide, ck_v[head], (((1,), (1,)), ((), ())), preferred_element_type=f32
+        )
+        scores = jnp.where(head_row == head, part, scores)
+    scale = head_dim ** (-0.5)
+    own_score = jnp.sum(q_unit * k_unit, axis=-1, keepdims=True) * scale
+    live = lax.broadcasted_iota(jnp.int32, (maps, cache_len), 1) < lengths[0]
+    scores = jnp.where(live, scores * scale, masked_score)
+    peak = jnp.maximum(jnp.max(scores, axis=-1, keepdims=True), own_score)
+    past_weight = jnp.exp(scores - peak)
+    own_weight = jnp.exp(own_score - peak)
+    totals = jnp.sum(past_weight, axis=-1, keepdims=True) + own_weight
+    past_prob = past_weight / totals
+    own_prob = own_weight / totals
+    lam = jnp.zeros((kv_heads, 1), f32)
+    for head in range(kv_heads):
+        lam = jnp.where(row[:kv_heads] == head, lambdas[head], lam)
+    past_mix = (past_prob[:kv_heads] - lam * past_prob[kv_heads:]).astype(bf16)
+    own_mix = (own_prob[:kv_heads] - lam * own_prob[kv_heads:]).astype(bf16).astype(f32)
+    cv_c.wait()
+    head_out = jnp.zeros((kv_heads, key_width), f32)
+    for head in range(kv_heads):
+        part = jnp.dot(past_mix, cv_v[head], preferred_element_type=f32)
+        head_out = jnp.where(row[:kv_heads] == head, part, head_out)
+    head_out = head_out + own_mix * value_own
+    mixed = (head_out * rms_scale(head_out) * sub_gain_v[...] * out_factor).astype(bf16)
+    mix_all[tp] = mixed.astype(f32)
+    for step in range(1, n_tp):
+        tp_copy(step, lambda peer: mix_all.at[tp], mix_all, mix_s, mix_r).start()
+    wo_c.wait()
+    for step in range(1, n_tp):
+        tp_wait(step, mix_all, mix_s, mix_r).wait_recv()
+    mixed_rows = jnp.concatenate([mix_all[:, head, :] for head in range(kv_heads)], axis=1)
+    attn_proj = jnp.dot(mixed_rows.astype(bf16), wo_v[...], preferred_element_type=f32)
+    updated = (res_all[tp].astype(f32) + attn_proj).astype(bf16)
+    upd_all[me] = updated
+
+    def any_copy(other, source, target, send, recv):
+        return pltpu.make_async_remote_copy(
+            src_ref=source,
+            dst_ref=target.at[me],
+            send_sem=send.at[other],
+            recv_sem=recv.at[me],
+            device_id=(other // n_tp, lax.rem(other, n_tp)),
+            device_id_type=MESH,
+        )
+
+    def any_wait(other, target, send, recv):
+        return pltpu.make_async_remote_copy(
+            src_ref=target.at[other],
+            dst_ref=target.at[other],
+            send_sem=send.at[other],
+            recv_sem=recv.at[other],
+            device_id=(other // n_tp, lax.rem(other, n_tp)),
+            device_id_type=MESH,
+        )
+
+    def upd_start(step, carry):
+        any_copy(lax.rem(me + step, count), upd_all.at[me], upd_all, upd_s, upd_r).start()
+        return carry
+
+    lax.fori_loop(1, count, upd_start, 0)
+
+    def upd_wait(step, carry):
+        any_wait(lax.rem(me + step, count), upd_all, upd_s, upd_r).wait_recv()
+        return carry
+
+    wg_c.wait()
+    wu_c.wait()
+    wd_c.wait()
+    lax.fori_loop(1, count, upd_wait, 0)
+    for e in range(n_ep):
+        for t in range(n_tp):
+            rows_v[e * group : (e + 1) * group, t * width : (t + 1) * width] = upd_all[
+                e * n_tp + t
+            ].astype(f32)
+    rows = rows_v[...]
+    hidden = (rows * rms_scale(rows) * ffn_gain_v[...]).astype(bf16)
+    gate_out = jnp.dot(hidden, wg_v[...], preferred_element_type=f32)
+    up_out = jnp.dot(hidden, wu_v[...], preferred_element_type=f32)
+    act = (jax.nn.silu(gate_out) * up_out).astype(bf16)
+
+    for t in range(n_tp):
+        slab = jnp.dot(act, wd_v[:, t * width : (t + 1) * width], preferred_element_type=f32)
+        for e in range(n_ep):
+            part_send[e * n_tp + t] = slab[e * group : (e + 1) * group].astype(bf16)
+
+        def part_start(step, carry):
+            other = lax.rem(ep + step, n_ep) * n_tp + t
+
+            @pl.when(other != me)
+            def _():
+                any_copy(other, part_send.at[other], part_all, part_s, part_r).start()
+
+            return carry
+
+        lax.fori_loop(0, n_ep, part_start, 0)
+    part_all[me] = part_send[me]
+
+    def part_wait(step, carry):
+        any_wait(lax.rem(me + step, count), part_all, part_s, part_r).wait_recv()
+        return carry
+
+    lax.fori_loop(1, count, part_wait, 0)
+    expert_mix = jnp.zeros((group, width), f32)
+    for e in range(n_ep):
+        term = part_all[e * n_tp].astype(f32)
+        for t in range(1, n_tp):
+            term = term + part_all[e * n_tp + t].astype(f32)
+        share = jnp.sum(jnp.where(routes_v[...] == e, weights_v[...], 0.0), axis=1, keepdims=True)
+        expert_mix = expert_mix + share * term
+    result_v[...] = (upd_all[me].astype(f32) + expert_mix).astype(bf16)
+    out_copies.append(pltpu.make_async_copy(result_v, result, out_sem.at[2]))
+    out_copies[2].start()
+
+    for step in range(1, n_tp):
+        tp_wait(step, res_all, res_s, res_r).wait_send()
+        tp_wait(step, proj_all, proj_s, proj_r).wait_send()
+        tp_wait(step, mix_all, mix_s, mix_r).wait_send()
+
+    def drain(step, carry):
+        other = lax.rem(me + step, count)
+        any_wait(other, upd_all, upd_s, upd_r).wait_send()
+        any_wait(other, part_all, part_s, part_r).wait_send()
+        return carry
+
+    lax.fori_loop(1, count, drain, 0)
+    for copy in out_copies:
+        copy.wait()
+
+
+def fused_layer(n_ep, n_tp, *args):
+    (
+        resid,
+        cache_key,
+        cache_value,
+        lengths,
+        lambdas,
+        mix_gain,
+        query_gain,
+        key_gain,
+        sub_gain,
+        ffn_gain,
+        w_query,
+        w_key,
+        w_value,
+        w_out,
+        routes,
+        route_weights,
+        w_gate,
+        w_up,
+        w_down,
+    ) = args
+    bf16, f32 = jnp.bfloat16, jnp.float32
+    group, width = resid.shape
+    _, kv_heads, cache_len, key_width = cache_key.shape
+    head_dim = key_width // 2
+    features = width * n_tp
+    hidden_units = w_gate.shape[2]
+    count = n_ep * n_tp
+    blocks = 6 * (width // key_width)
+    any_spec = pl.BlockSpec(memory_space=pl.ANY)
+    smem_spec = pl.BlockSpec(memory_space=pltpu.SMEM)
+    operands = (
+        lengths,
+        lambdas,
+        resid,
+        mix_gain.reshape(1, -1),
+        query_gain.reshape(1, -1),
+        key_gain.reshape(1, -1),
+        sub_gain.reshape(1, -1),
+        ffn_gain.reshape(1, -1),
+        routes,
+        route_weights,
+        w_query,
+        w_key,
+        w_value,
+        cache_key,
+        cache_value,
+        w_out,
+        w_gate,
+        w_up,
+        w_down,
+    )
+    dma = pltpu.SemaphoreType.DMA
+    return pl.pallas_call(
+        functools.partial(fused, n_ep, n_tp),
+        out_shape=(
+            jax.ShapeDtypeStruct((group, width), bf16),
+            jax.ShapeDtypeStruct((1, kv_heads, key_width), bf16),
+            jax.ShapeDtypeStruct((1, kv_heads, key_width), bf16),
+        ),
+        in_specs=[smem_spec] * 2 + [any_spec] * (len(operands) - 2),
+        out_specs=(any_spec,) * 3,
+        scratch_shapes=[
+            pltpu.VMEM((1, features), f32),
+            pltpu.VMEM((1, head_dim), f32),
+            pltpu.VMEM((1, head_dim), f32),
+            pltpu.VMEM((1, key_width), f32),
+            pltpu.VMEM((1, features), f32),
+            pltpu.VMEM(routes.shape, jnp.int32),
+            pltpu.VMEM(routes.shape, f32),
+            pltpu.VMEM((features, width), bf16),
+            pltpu.VMEM((features, width), bf16),
+            pltpu.VMEM((features, width), bf16),
+            pltpu.VMEM((kv_heads, cache_len, key_width), bf16),
+            pltpu.VMEM((kv_heads, cache_len, key_width), bf16),
+            pltpu.VMEM((features, width), bf16),
+            pltpu.VMEM((features, hidden_units), bf16),
+            pltpu.VMEM((features, hidden_units), bf16),
+            pltpu.VMEM((hidden_units, features), bf16),
+            pltpu.VMEM((n_tp, group, width), bf16),
+            pltpu.VMEM((n_tp, blocks, head_dim), f32),
+            pltpu.VMEM((n_tp, blocks, head_dim), f32),
+            pltpu.VMEM((3, 2, kv_heads, head_dim), f32),
+            pltpu.VMEM((n_tp, kv_heads, key_width), f32),
+            pltpu.VMEM((count, group, width), bf16),
+            pltpu.VMEM((n_ep * group, features), f32),
+            pltpu.VMEM((count, group, width), bf16),
+            pltpu.VMEM((count, group, width), bf16),
+            pltpu.VMEM((group, width), bf16),
+            pltpu.VMEM((kv_heads, key_width), bf16),
+            pltpu.VMEM((kv_heads, key_width), bf16),
+            dma((17,)),
+            dma((3,)),
+        ]
+        + [dma((n_tp,))] * 6
+        + [dma((count,))] * 4,
+        compiler_params=pltpu.CompilerParams(
+            collective_id=0, has_side_effects=True, vmem_limit_bytes=60 * 1024 * 1024
+        ),
+        name="fused_layer",
+    )(*operands)
+
+
+def layer(n_ep, n_tp, *args):
+    resid, cache_key, lambdas, w_gate = args[0], args[1], args[4], args[16]
+    group, width = resid.shape
+    sequences, kv_heads, _, key_width = cache_key.shape
+    aligned = (
+        sequences == 1
+        and group == n_tp
+        and n_tp > 1
+        and lambdas.shape[0] == kv_heads
+        and kv_heads % 8 == 0
+        and key_width % 256 == 0
+        and width % key_width == 0
+        and w_gate.shape[0] == 1
+        and n_ep * n_tp <= 32
+    )
+    if aligned:
+        return fused_layer(n_ep, n_tp, *args)
+    return local(*args)
+
+
 def solution(mesh):
     in_specs = (
         P("ep", "tp"),
@@ -196,4 +675,4 @@
         P("ep", "tp", None),
     )
     out_specs = (P("ep", "tp"), P(("ep", "tp"), None, None), P(("ep", "tp"), None, None))
-    return jax.shard_map(local, mesh=mesh, in_specs=in_specs, out_specs=out_specs, check_vma=False)
+    return jax.shard_map(functools.partial(layer, mesh.shape["ep"], mesh.shape["tp"]), mesh=mesh, in_specs=in_specs, out_specs=out_specs, check_vma=False)

time: 131 us -> 40.9 us (0.31)
  blocking collectives: 36.7 us -> 0 us
  waiting for transfers between devices: 34.4 us -> 0 us
  Pallas kernels: 0 us -> 32.9 us
  matrix products: 16.3 us -> 0 us
  starting transfers between devices: 15.3 us -> 0 us
  between operations: 15 us -> 1.29 us
  other arithmetic: 4.59 us -> 0 us
    pallas_call x0 -> x1, Pallas kernels: none -> 32.9 us  [fused_layer(): pl.pallas_call(functools.partial(fused, n_ep, n_tp), out_shape=(jax.Shape...]
    all_gather x3 -> x0, blocking collectives: 25.3 us -> none  [the longest x1 9.93 us: local(): gathered = lax.all_gather(resid, 'tp', axis=1, tiled=True)]
    reduce_scatter x1 -> x0, waiting for transfers between devices: 22.2 us -> none  [local(): lax.psum_scatter(partial_value.astype(jnp.bfloat16), 'tp', scatter_dimens...]
    dot_general x11 -> x0, matrix products: 16.3 us -> none  [the longest x1 3.62 us: local(): down_out = jnp.dot(act, w_down[0], preferred_element_type=jnp.float32)]
    all_to_all x4 -> x0, starting transfers between devices: 15.2 us -> none  [the longest x1 4.6 us: local(): lax.all_to_all(summed.astype(jnp.bfloat16), 'ep', split_axis=0, concat_ax...]
    all_to_all x4 -> x0, waiting for transfers between devices: 12.2 us -> none  [the longest x1 4.63 us: local(): lax.all_to_all(key_part, 'tp', split_axis=0, concat_axis=1, tiled=True)]
    all_to_all x1 -> x0, blocking collectives: 11.4 us -> none  [local(): slots = lax.all_to_all(send, 'ep', split_axis=0, concat_axis=0, tiled=True)]
    unnamed x33 -> x5, local copies, waits for them, and re-layouts: 2.38 us -> 6.47 us
  transfers between devices with their start and end apart: 5 -> 0, of which waited for: 4 -> 0; matrix products, arithmetic and copies ran while one was open for 9% -> 0% of each run, Pallas kernels for 0% -> 0%
where the time goes in v1:
time: 40.9 us; the launch traced here: 40.7 us
  Pallas kernels  32.9 us (80%)
  local copies, waits for them, and re-layouts  6.47 us (16%)
  between operations  1.29 us (3%)
    pallas_call x1, Pallas kernels, fused_layer(): pl.pallas_call(functools.partial(fused, n_ep, n_tp), out_shape=(jax.Shape...  32.9 us
    unnamed x5, local copies, waits for them, and re-layouts  6.47 us

profile of v1, /device:TPU:0, one launch (start us, length us, event | category | flops | bytes accessed | tf_op | source)
XLA Modules:
  0.0 40.7 jit_solution(17696418323231431134)
XLA Ops:
  1.3 1.3 %copy.22.routes = s32[4,2]{1,0:T(4,128)} copy(s32[4,2]{0,1:T(2,128)} %param.33) | data formatting | bytes 64 | tf_op args[14]
  2.6 1.3 %copy.23.route_weights = f32[4,2]{1,0:T(4,128)} copy(f32[4,2]{0,1:T(2,128)} %param.34) | data formatting | bytes 64 | tf_op args[15]
  3.9 32.9 %fused_layer.1 = (bf16[4,512]{1,0:T(4,128)(2,1)}, bf16[1,8,256]{2,1,0:T(8,128)(2,1)}, bf16[1,8,256]{2,1,0:T(8,128)(2,1)}) custom-call(s32[1]{0:T(128)S(6)} %copy.27.lengths, f32[8]{0:T(128)} %lambdas.1, bf16[4,512]{1,0:T(4,128)(2,1)} %resid.1, f32[1,2048]{1,0:T(1,128)} %bitcast.5, f32[1,128]{1,0:T(1,128)} %bitcast.8, f32[1,128]{1,0:T(1,128)} %bitcast.9, ...), custom_call_target="tpu_custom_call" | custom-call | tf_op jit(solution)/shard_map/fused_layer/pallas_call | solution.py:585
  36.9 1.3 %copy.28 = bf16[4,512]{1,0:T(4,128)(2,1)} copy(bf16[4,512]{1,0:T(4,128)(2,1)} %get-tuple-element.6) | data formatting | bytes 8192
  38.1 1.3 %copy.29 = bf16[1,8,256]{2,1,0:T(8,128)(2,1)} copy(bf16[1,8,256]{2,1,0:T(8,128)(2,1)} %get-tuple-element.7) | data formatting | bytes 8192
  39.4 1.3 %copy.30 = bf16[1,8,256]{2,1,0:T(8,128)(2,1)} copy(bf16[1,8,256]{2,1,0:T(8,128)(2,1)} %get-tuple-element.8) | data formatting | bytes 8192

commit v2 on v1

--- a/solution.py
+++ b/solution.py
@@ -213,6 +213,8 @@
     key_gain_v,
     sub_gain_v,
     ffn_gain_v,
+    lengths_v,
+    lambdas_v,
     routes_v,
     weights_v,
     wq_v,
@@ -268,6 +270,8 @@
         (key_gain, key_gain_v),
         (sub_gain, sub_gain_v),
         (ffn_gain, ffn_gain_v),
+        (lengths, lengths_v),
+        (lambdas, lambdas_v),
         (routes, routes_v),
         (route_weights, weights_v),
         (cache_key.at[0], ck_v),
@@ -281,7 +285,7 @@
         pltpu.make_async_copy(source, target, load_sem.at[at])
         for at, (source, target) in enumerate(loads)
     ]
-    for copy in copies:
+    for copy in copies[:5]:
         copy.start()
     (
         resid_c,
@@ -293,6 +297,8 @@
         key_gain_c,
         sub_gain_c,
         ffn_gain_c,
+        lengths_c,
+        lambdas_c,
         routes_c,
         weights_c,
         ck_c,
@@ -305,18 +311,17 @@
 
     barrier = pltpu.get_barrier_semaphore()
 
-    def greet(step, carry):
-        other = lax.rem(me + step, count)
+    for step in range(1, n_tp):
         pl.semaphore_signal(
-            barrier,
-            inc=1,
-            device_id=(other // n_tp, lax.rem(other, n_tp)),
-            device_id_type=MESH,
+            barrier, inc=1, device_id=(ep, lax.rem(tp + step, n_tp)), device_id_type=MESH
         )
-        return carry
-
-    lax.fori_loop(1, count, greet, 0)
-    pl.semaphore_wait(barrier, count - 1)
+    for step in range(1, n_ep):
+        pl.semaphore_signal(
+            barrier, inc=1, device_id=(lax.rem(ep + step, n_ep), tp), device_id_type=MESH
+        )
+    for copy in copies[5:]:
+        copy.start()
+    pl.semaphore_wait(barrier, n_tp + n_ep - 2)
 
     def tp_copy(step, source, target, send, recv):
         peer = lax.rem(tp + step, n_tp)
@@ -362,7 +367,7 @@
     for step in range(1, n_tp):
         tp_copy(step, lambda peer: proj_send.at[peer], proj_all, proj_s, proj_r).start()
     proj_all[tp] = proj_send[tp]
-    for copy in (query_gain_c, key_gain_c, sub_gain_c, ffn_gain_c, routes_c, weights_c):
+    for copy in (query_gain_c, key_gain_c, sub_gain_c, ffn_gain_c, lengths_c, lambdas_c, routes_c, weights_c):
         copy.wait()
     for step in range(1, n_tp):
         tp_wait(step, proj_all, proj_s, proj_r).wait_recv()
@@ -403,7 +408,7 @@
         scores = jnp.where(head_row == head, part, scores)
     scale = head_dim ** (-0.5)
     own_score = jnp.sum(q_unit * k_unit, axis=-1, keepdims=True) * scale
-    live = lax.broadcasted_iota(jnp.int32, (maps, cache_len), 1) < lengths[0]
+    live = lax.broadcasted_iota(jnp.int32, (maps, cache_len), 1) < lengths_v[0]
     scores = jnp.where(live, scores * scale, masked_score)
     peak = jnp.maximum(jnp.max(scores, axis=-1, keepdims=True), own_score)
     past_weight = jnp.exp(scores - peak)
@@ -413,7 +418,7 @@
     own_prob = own_weight / totals
     lam = jnp.zeros((kv_heads, 1), f32)
     for head in range(kv_heads):
-        lam = jnp.where(row[:kv_heads] == head, lambdas[head], lam)
+        lam = jnp.where(row[:kv_heads] == head, lambdas_v[head], lam)
     past_mix = (past_prob[:kv_heads] - lam * past_prob[kv_heads:]).astype(bf16)
     own_mix = (own_prob[:kv_heads] - lam * own_prob[kv_heads:]).astype(bf16).astype(f32)
     cv_c.wait()
@@ -434,23 +439,32 @@
     updated = (res_all[tp].astype(f32) + attn_proj).astype(bf16)
     upd_all[me] = updated
 
+    token = lax.broadcasted_iota(jnp.int32, (group, 128), 0)
+    expert = lax.broadcasted_iota(jnp.int32, (group, 128), 1)
+    shares = jnp.zeros((group, 128), f32)
+    for s in range(group):
+        for k in range(2):
+            named = jnp.logical_and(token == s, expert == routes_v[k, s])
+            shares = jnp.where(named, weights_v[k, s], shares)
+
     def any_copy(other, source, target, send, recv):
         return pltpu.make_async_remote_copy(
             src_ref=source,
             dst_ref=target.at[me],
-            send_sem=send.at[other],
-            recv_sem=recv.at[me],
+            send_sem=send,
+            recv_sem=recv,
             device_id=(other // n_tp, lax.rem(other, n_tp)),
             device_id_type=MESH,
         )
 
-    def any_wait(other, target, send, recv):
+    def any_wait(target, send, recv):
+        span = target.at[pl.ds(0, count - 1)]
         return pltpu.make_async_remote_copy(
-            src_ref=target.at[other],
-            dst_ref=target.at[other],
-            send_sem=send.at[other],
-            recv_sem=recv.at[other],
-            device_id=(other // n_tp, lax.rem(other, n_tp)),
+            src_ref=span,
+            dst_ref=span,
+            send_sem=send,
+            recv_sem=recv,
+            device_id=(ep, tp),
             device_id_type=MESH,
         )
 
@@ -460,14 +474,10 @@
 
     lax.fori_loop(1, count, upd_start, 0)
 
-    def upd_wait(step, carry):
-        any_wait(lax.rem(me + step, count), upd_all, upd_s, upd_r).wait_recv()
-        return carry
-
     wg_c.wait()
     wu_c.wait()
     wd_c.wait()
-    lax.fori_loop(1, count, upd_wait, 0)
+    any_wait(upd_all, upd_s, upd_r).wait_recv()
     for e in range(n_ep):
         for t in range(n_tp):
             rows_v[e * group : (e + 1) * group, t * width : (t + 1) * width] = upd_all[
@@ -496,18 +506,13 @@
         lax.fori_loop(0, n_ep, part_start, 0)
     part_all[me] = part_send[me]
 
-    def part_wait(step, carry):
-        any_wait(lax.rem(me + step, count), part_all, part_s, part_r).wait_recv()
-        return carry
-
-    lax.fori_loop(1, count, part_wait, 0)
+    any_wait(part_all, part_s, part_r).wait_recv()
     expert_mix = jnp.zeros((group, width), f32)
     for e in range(n_ep):
         term = part_all[e * n_tp].astype(f32)
         for t in range(1, n_tp):
             term = term + part_all[e * n_tp + t].astype(f32)
-        share = jnp.sum(jnp.where(routes_v[...] == e, weights_v[...], 0.0), axis=1, keepdims=True)
-        expert_mix = expert_mix + share * term
+        expert_mix = expert_mix + shares[:, e : e + 1] * term
     result_v[...] = (upd_all[me].astype(f32) + expert_mix).astype(bf16)
     out_copies.append(pltpu.make_async_copy(result_v, result, out_sem.at[2]))
     out_copies[2].start()
@@ -517,15 +522,15 @@
         tp_wait(step, proj_all, proj_s, proj_r).wait_send()
         tp_wait(step, mix_all, mix_s, mix_r).wait_send()
 
-    def drain(step, carry):
-        other = lax.rem(me + step, count)
-        any_wait(other, upd_all, upd_s, upd_r).wait_send()
-        any_wait(other, part_all, part_s, part_r).wait_send()
-        return carry
-
-    lax.fori_loop(1, count, drain, 0)
+    any_wait(upd_all, upd_s, upd_r).wait_send()
+    any_wait(part_all, part_s, part_r).wait_send()
     for copy in out_copies:
         copy.wait()
+
+
+def hand_over(*refs):
+    for source, target in zip(refs[:3], refs[3:]):
+        target[...] = source[...]
 
 
 def fused_layer(n_ep, n_tp, *args):
@@ -559,7 +564,6 @@
     count = n_ep * n_tp
     blocks = 6 * (width // key_width)
     any_spec = pl.BlockSpec(memory_space=pl.ANY)
-    smem_spec = pl.BlockSpec(memory_space=pltpu.SMEM)
     operands = (
         lengths,
         lambdas,
@@ -569,8 +573,8 @@
         key_gain.reshape(1, -1),
         sub_gain.reshape(1, -1),
         ffn_gain.reshape(1, -1),
-        routes,
-        route_weights,
+        routes.T,
+        route_weights.T,
         w_query,
         w_key,
         w_value,
@@ -582,14 +586,14 @@
         w_down,
     )
     dma = pltpu.SemaphoreType.DMA
-    return pl.pallas_call(
+    outs = pl.pallas_call(
         functools.partial(fused, n_ep, n_tp),
         out_shape=(
             jax.ShapeDtypeStruct((group, width), bf16),
             jax.ShapeDtypeStruct((1, kv_heads, key_width), bf16),
             jax.ShapeDtypeStruct((1, kv_heads, key_width), bf16),
         ),
-        in_specs=[smem_spec] * 2 + [any_spec] * (len(operands) - 2),
+        in_specs=[any_spec] * len(operands),
         out_specs=(any_spec,) * 3,
         scratch_shapes=[
             pltpu.VMEM((1, features), f32),
@@ -597,8 +601,10 @@
             pltpu.VMEM((1, head_dim), f32),
             pltpu.VMEM((1, key_width), f32),
             pltpu.VMEM((1, features), f32),
-            pltpu.VMEM(routes.shape, jnp.int32),
-            pltpu.VMEM(routes.shape, f32),
+            pltpu.SMEM(lengths.shape, jnp.int32),
+            pltpu.SMEM(lambdas.shape, f32),
+            pltpu.SMEM(routes.shape[::-1], jnp.int32),
+            pltpu.SMEM(routes.shape[::-1], f32),
             pltpu.VMEM((features, width), bf16),
             pltpu.VMEM((features, width), bf16),
             pltpu.VMEM((features, width), bf16),
@@ -620,16 +626,23 @@
             pltpu.VMEM((group, width), bf16),
             pltpu.VMEM((kv_heads, key_width), bf16),
             pltpu.VMEM((kv_heads, key_width), bf16),
-            dma((17,)),
+            dma((19,)),
             dma((3,)),
         ]
         + [dma((n_tp,))] * 6
-        + [dma((count,))] * 4,
+        + [dma] * 4,
         compiler_params=pltpu.CompilerParams(
             collective_id=0, has_side_effects=True, vmem_limit_bytes=60 * 1024 * 1024
         ),
         name="fused_layer",
     )(*operands)
+    return pl.pallas_call(
+        hand_over,
+        out_shape=tuple(jax.ShapeDtypeStruct(out.shape, out.dtype) for out in outs),
+        in_specs=[pl.BlockSpec(memory_space=pltpu.VMEM)] * 3,
+        out_specs=(pl.BlockSpec(memory_space=pltpu.VMEM),) * 3,
+        name="hand_over",
+    )(*outs)
 
 
 def layer(n_ep, n_tp, *args):

time: 40.9 us -> 33.7 us (0.82)
  local copies, waits for them, and re-layouts: 6.47 us -> 0 us
  Pallas kernels: 32.9 us -> 32.3 us
    unnamed x5 -> x0, local copies, waits for them, and re-layouts: 6.47 us -> none
    pallas_call x1, Pallas kernels: 32.9 us -> 31 us  [fused_layer(): pl.pallas_call(functools.partial(fused, n_ep, n_tp), out_shape=(jax.Shape...]
    pallas_call x0 -> x1, Pallas kernels: none -> 1.3 us  [fused_layer(): pl.pallas_call(hand_over, out_shape=tuple((jax.ShapeDtypeStruct(out.shape...]
where the time goes in v2:
time: 33.7 us; the launch traced here: 33.6 us
  Pallas kernels  32.3 us (96%)
  between operations  1.29 us (4%)
    pallas_call x1, Pallas kernels, fused_layer(): pl.pallas_call(functools.partial(fused, n_ep, n_tp), out_shape=(jax.Shape...  31 us
    pallas_call x1, Pallas kernels, fused_layer(): pl.pallas_call(hand_over, out_shape=tuple((jax.ShapeDtypeStruct(out.shape...  1.3 us

profile of v2, /device:TPU:0, one launch (start us, length us, event | category | flops | bytes accessed | tf_op | source)
XLA Modules:
  0.0 33.6 jit_solution(5893788185600358786)
XLA Ops:
  1.3 31.0 %fused_layer.1 = (bf16[4,512]{1,0:T(4,128)(2,1)}, bf16[1,8,256]{2,1,0:T(8,128)(2,1)}, bf16[1,8,256]{2,1,0:T(8,128)(2,1)}) custom-call(s32[1]{0:T(128)S(6)} %copy.22.lengths, f32[8]{0:T(128)} %lambdas.1, bf16[4,512]{1,0:T(4,128)(2,1)} %resid.1, f32[1,2048]{1,0:T(1,128)} %bitcast.7, f32[1,128]{1,0:T(1,128)} %bitcast.12, f32[1,128]{1,0:T(1,128)} %bitcast.13, ...), custom_call_target="tpu_custom_call" | custom-call | tf_op jit(solution)/shard_map/fused_layer/pallas_call | solution.py:589
  32.3 1.3 %hand_over.1 = (bf16[4,512]{1,0:T(4,128)(2,1)}, bf16[1,8,256]{2,1,0:T(8,128)(2,1)}, bf16[1,8,256]{2,1,0:T(8,128)(2,1)}) custom-call(bf16[4,512]{1,0:T(4,128)(2,1)} %get-tuple-element.6.refs_0_, bf16[1,8,256]{2,1,0:T(8,128)(2,1)} %get-tuple-element.7.refs_1_, bf16[1,8,256]{2,1,0:T(8,128)(2,1)} %get-tuple-element.8.refs_2_), custom_call_target="tpu_custom_call" | custom-call | tf_op jit(solution)/shard_map/hand_over/pallas_call | solution.py:639

commit v3 on v2

--- a/solution.py
+++ b/solution.py
@@ -428,13 +428,14 @@
         head_out = jnp.where(row[:kv_heads] == head, part, head_out)
     head_out = head_out + own_mix * value_own
     mixed = (head_out * rms_scale(head_out) * sub_gain_v[...] * out_factor).astype(bf16)
-    mix_all[tp] = mixed.astype(f32)
+    mix_all[tp] = mixed
     for step in range(1, n_tp):
         tp_copy(step, lambda peer: mix_all.at[tp], mix_all, mix_s, mix_r).start()
     wo_c.wait()
     for step in range(1, n_tp):
         tp_wait(step, mix_all, mix_s, mix_r).wait_recv()
-    mixed_rows = jnp.concatenate([mix_all[:, head, :] for head in range(kv_heads)], axis=1)
+    mixed_wide = mix_all[...].astype(f32)
+    mixed_rows = jnp.concatenate([mixed_wide[:, head, :] for head in range(kv_heads)], axis=1)
     attn_proj = jnp.dot(mixed_rows.astype(bf16), wo_v[...], preferred_element_type=f32)
     updated = (res_all[tp].astype(f32) + attn_proj).astype(bf16)
     upd_all[me] = updated
@@ -469,7 +470,7 @@
         )
 
     def upd_start(step, carry):
-        any_copy(lax.rem(me + step, count), upd_all.at[me], upd_all, upd_s, upd_r).start()
+        any_copy(lax.rem(me + count - step, count), upd_all.at[me], upd_all, upd_s, upd_r).start()
         return carry
 
     lax.fori_loop(1, count, upd_start, 0)
@@ -495,7 +496,7 @@
             part_send[e * n_tp + t] = slab[e * group : (e + 1) * group].astype(bf16)
 
         def part_start(step, carry):
-            other = lax.rem(ep + step, n_ep) * n_tp + t
+            other = lax.rem(ep + n_ep - 1 - step, n_ep) * n_tp + t
 
             @pl.when(other != me)
             def _():
@@ -618,7 +619,7 @@
             pltpu.VMEM((n_tp, blocks, head_dim), f32),
             pltpu.VMEM((n_tp, blocks, head_dim), f32),
             pltpu.VMEM((3, 2, kv_heads, head_dim), f32),
-            pltpu.VMEM((n_tp, kv_heads, key_width), f32),
+            pltpu.VMEM((n_tp, kv_heads, key_width), bf16),
             pltpu.VMEM((count, group, width), bf16),
             pltpu.VMEM((n_ep * group, features), f32),
             pltpu.VMEM((count, group, width), bf16),

time: 33.7 us -> 33.2 us (0.985)
  Pallas kernels: 32.3 us -> 31.7 us
    pallas_call x1, Pallas kernels: 31 us -> 30.4 us  [fused_layer(): pl.pallas_call(functools.partial(fused, n_ep, n_tp), out_shape=(jax.Shape...]
where the time goes in v3:
time: 33.2 us; the launch traced here: 33 us
  Pallas kernels  31.7 us (95%)
  between operations  1.29 us (4%)
    pallas_call x1, Pallas kernels, fused_layer(): pl.pallas_call(functools.partial(fused, n_ep, n_tp), out_shape=(jax.Shape...  30.4 us
    pallas_call x1, Pallas kernels, fused_layer(): pl.pallas_call(hand_over, out_shape=tuple((jax.ShapeDtypeStruct(out.shape...  1.3 us

profile of v3, /device:TPU:0, one launch (start us, length us, event | category | flops | bytes accessed | tf_op | source)
XLA Modules:
  0.0 33.0 jit_solution(15215475916495227392)
XLA Ops:
  1.3 30.4 %fused_layer.1 = (bf16[4,512]{1,0:T(4,128)(2,1)}, bf16[1,8,256]{2,1,0:T(8,128)(2,1)}, bf16[1,8,256]{2,1,0:T(8,128)(2,1)}) custom-call(s32[1]{0:T(128)S(6)} %copy.22.lengths, f32[8]{0:T(128)} %lambdas.1, bf16[4,512]{1,0:T(4,128)(2,1)} %resid.1, f32[1,2048]{1,0:T(1,128)} %bitcast.7, f32[1,128]{1,0:T(1,128)} %bitcast.12, f32[1,128]{1,0:T(1,128)} %bitcast.13, ...), custom_call_target="tpu_custom_call" | custom-call | tf_op jit(solution)/shard_map/fused_layer/pallas_call | solution.py:590
  31.7 1.3 %hand_over.1 = (bf16[4,512]{1,0:T(4,128)(2,1)}, bf16[1,8,256]{2,1,0:T(8,128)(2,1)}, bf16[1,8,256]{2,1,0:T(8,128)(2,1)}) custom-call(bf16[4,512]{1,0:T(4,128)(2,1)} %get-tuple-element.6.refs_0_, bf16[1,8,256]{2,1,0:T(8,128)(2,1)} %get-tuple-element.7.refs_1_, bf16[1,8,256]{2,1,0:T(8,128)(2,1)} %get-tuple-element.8.refs_2_), custom_call_target="tpu_custom_call" | custom-call | tf_op jit(solution)/shard_map/hand_over/pallas_call | solution.py:640
